TPU v7x, 32 devices: a whole 2x2x4 slice. The times are simulated.
32 devices in a mesh: sp: 8 (over z, y), tp: 4 (over x, core).
Axes of the slice: x: 2, y: 2, z: 4, core: 2. Of those that a mesh axis runs over, the one named last changes fastest.
Arguments:
- resid: bfloat16 [1536, 2048], P('sp'), may hold values from -6 to 6
- query_broad: bfloat16 [1536, 1536], P('sp', 'tp'), may hold values from -60 to 60
- query_narrow: bfloat16 [1536, 1024], P('sp', 'tp'), may hold values from -60 to 60
- latent: bfloat16 [1536, 512], P('sp'), may hold values from -6 to 6
- key_rope: bfloat16 [1536, 64], P('sp'), may hold values from -6 to 6
- latent_gain: float32 [512], replicated, may hold values from 0.1 to 1.9
- key_up_broad: bfloat16 [512, 1024], P(None, 'tp'), may hold values from -0.25 to 0.25
- value_up_broad: bfloat16 [512, 1024], P(None, 'tp'), may hold values from -0.25 to 0.25
- key_up_narrow: bfloat16 [512, 512], P(None, 'tp'), may hold values from -0.25 to 0.25
- value_up_narrow: bfloat16 [512, 512], P(None, 'tp'), may hold values from -0.25 to 0.25
- out_broad: bfloat16 [1024, 2048], replicated, may hold values from -0.15625 to 0.15625
- out_narrow: bfloat16 [512, 2048], replicated, may hold values from -0.15625 to 0.15625
- post_gain: float32 [2048], replicated, may hold values from 0.1 to 1.9
- ffn_gain: float32 [2048], replicated, may hold values from 0.1 to 1.9
- up_weight: bfloat16 [2048, 8192], P('sp', 'tp'), may hold values from -0.125 to 0.125
- down_weight: bfloat16 [2048, 8192], P('sp', 'tp'), may hold values from -0.0625 to 0.0625
- ffn_out_gain: float32 [2048], replicated, may hold values from 0.1 to 1.9
Outputs:
- layer_out: bfloat16 [1536, 2048], P(('sp', 'tp'))
All inputs are finite; a program needn't handle non-finite values.
Results may differ from a plain program's by a relative error of at most 0.013.
Values may be sent and summed in bfloat16 or wider, within the bound.
A program may use at most 128 MiB of HBM per device.

v0:
```python
import functools
import math

import jax
import jax.numpy as jnp
from jax import lax
from jax.experimental import pallas as pl
from jax.experimental.pallas import tpu as pltpu
from jax.sharding import PartitionSpec as P

DB = 128
DN = 64


norm_eps = 1e-06
rope_base = 500000.0
masked_score = -1e30


def rotate(values, positions):
    full_width = values.shape[-1]
    half_width = full_width // 2
    frequency = rope_base ** (-2.0 * jnp.arange(half_width, dtype=jnp.float32) / full_width)
    angles = positions.astype(jnp.float32)[:, None] * frequency[None, :]
    angle_shape = (angles.shape[0],) + (1,) * (values.ndim - 2) + (half_width,)
    cosine = jnp.cos(angles).reshape(angle_shape)
    sine_part = jnp.sin(angles).reshape(angle_shape)
    leading = values[..., :half_width]
    trailing = values[..., half_width:]
    return jnp.concatenate(
        [leading * cosine - trailing * sine_part, trailing * cosine + leading * sine_part], axis=-1
    )


def rms_scale(values, norm_gain):
    return (
        values * lax.rsqrt(jnp.mean(values * values, axis=-1, keepdims=True) + norm_eps) * norm_gain
    )


def group_update(
    running, nope_query, rope_query, key_rows, key_rot, value_rows, score_scale, allowed
):
    old_max, old_sum, old_acc = running
    scores = jnp.einsum("qhd,khd->hqk", nope_query, key_rows, preferred_element_type=jnp.float32)
    scores = scores + jnp.einsum(
        "qhd,kd->hqk", rope_query, key_rot, preferred_element_type=jnp.float32
    )
    scores = jnp.where(allowed, scores * score_scale, masked_score)
    new_max = jnp.maximum(old_max, jnp.max(scores, axis=-1))
    exponent = jnp.where(allowed, jnp.exp(scores - new_max[:, :, None]), 0.0)
    factor = jnp.exp(old_max - new_max)
    new_sum = old_sum * factor + jnp.sum(exponent, axis=-1)
    weighted = jnp.einsum(
        "hqk,khd->qhd",
        exponent.astype(jnp.bfloat16),
        value_rows,
        preferred_element_type=jnp.float32,
    )
    new_acc = old_acc * jnp.transpose(factor)[:, :, None] + weighted
    return (new_max, new_sum, new_acc)


def local(
    resid,
    query_broad,
    query_narrow,
    latent,
    key_rope,
    latent_gain,
    key_up_broad,
    value_up_broad,
    key_up_narrow,
    value_up_narrow,
    out_broad,
    out_narrow,
    post_gain,
    ffn_gain,
    up_weight,
    down_weight,
    ffn_out_gain,
):
    local_rows = resid.shape[0]
    head_parts = lax.axis_size("tp")
    share_rows = local_rows // head_parts
    row_offset = lax.axis_index("sp") * local_rows
    last_query = row_offset + local_rows - 1
    query_pos = row_offset + jnp.arange(local_rows, dtype=jnp.int32)
    rope_width = key_rope.shape[1]
    broad_count = key_up_broad.shape[1] // DB
    narrow_count = key_up_narrow.shape[1] // DN
    broad_heads = query_broad.reshape(local_rows, broad_count, DB + rope_width)
    broad_nope = broad_heads[:, :, :DB]
    broad_rope = rotate(broad_heads[:, :, DB:].astype(jnp.float32), query_pos).astype(jnp.bfloat16)
    narrow_heads = query_narrow.reshape(local_rows, narrow_count, DN + rope_width)
    narrow_nope = narrow_heads[:, :, :DN]
    narrow_rope = rotate(narrow_heads[:, :, DN:].astype(jnp.float32), query_pos).astype(
        jnp.bfloat16
    )
    broad_scale = (DB + rope_width) ** (-0.5)
    narrow_scale = (DN + rope_width) ** (-0.5)

    def attend(running, latent_rows, rope_rows, first_row):
        key_count = latent_rows.shape[0]
        key_pos = first_row + jnp.arange(key_count, dtype=jnp.int32)
        latent_normed = rms_scale(latent_rows.astype(jnp.float32), latent_gain).astype(jnp.bfloat16)

        def expand(weight, head_size):
            product = jnp.dot(latent_normed, weight, preferred_element_type=jnp.float32)
            return product.astype(jnp.bfloat16).reshape(key_count, -1, head_size)

        key_rot = rotate(rope_rows.astype(jnp.float32), key_pos).astype(jnp.bfloat16)
        allowed = (key_pos[None, :] <= query_pos[:, None])[None]
        broad_state = group_update(
            running[0],
            broad_nope,
            broad_rope,
            expand(key_up_broad, DB),
            key_rot,
            expand(value_up_broad, DB),
            broad_scale,
            allowed,
        )
        narrow_state = group_update(
            running[1],
            narrow_nope,
            narrow_rope,
            expand(key_up_narrow, DN),
            key_rot,
            expand(value_up_narrow, DN),
            narrow_scale,
            allowed,
        )
        return (broad_state, narrow_state)

    def fresh(head_count, head_size):
        return (
            jnp.full((head_count, local_rows), masked_score, jnp.float32),
            jnp.zeros((head_count, local_rows), jnp.float32),
            jnp.zeros((local_rows, head_count, head_size), jnp.float32),
        )

    initial = (fresh(broad_count, DB), fresh(narrow_count, DN))
    latent_piece = lax.all_gather(latent, "sp", axis=0, tiled=True)
    rope_piece = lax.all_gather(key_rope, "sp", axis=0, tiled=True)
    piece_rows = latent_piece.shape[0]
    block_rows = math.gcd(piece_rows, 1024)

    def one_block(block_index, carried):
        begin = block_index * block_rows
        latent_block = lax.dynamic_slice_in_dim(latent_piece, begin, block_rows, 0)
        rope_block = lax.dynamic_slice_in_dim(rope_piece, begin, block_rows, 0)

        def unchanged(kept_state):
            return kept_state

        def updated(kept_state):
            return attend(kept_state, latent_block, rope_block, begin)

        return lax.cond(begin > last_query, unchanged, updated, carried)

    final_state = lax.fori_loop(0, piece_rows // block_rows, one_block, initial)

    def finish(running):
        run_max, run_sum, run_acc = running
        return (
            (run_acc / jnp.transpose(run_sum)[:, :, None])
            .astype(jnp.bfloat16)
            .reshape(local_rows, -1)
        )

    attn_broad = finish(final_state[0])
    attn_narrow = finish(final_state[1])
    rows_broad, rows_narrow = (
        lax.all_to_all(attn_broad, "tp", split_axis=0, concat_axis=1, tiled=True),
        lax.all_to_all(attn_narrow, "tp", split_axis=0, concat_axis=1, tiled=True),
    )
    projected = jnp.dot(rows_broad, out_broad, preferred_element_type=jnp.float32) + jnp.dot(
        rows_narrow, out_narrow, preferred_element_type=jnp.float32
    )
    own_resid = lax.dynamic_slice_in_dim(resid, lax.axis_index("tp") * share_rows, share_rows, 0)
    mixed = (own_resid.astype(jnp.float32) + rms_scale(projected, post_gain)).astype(jnp.bfloat16)
    normed = rms_scale(mixed.astype(jnp.float32), ffn_gain).astype(jnp.bfloat16)
    up_full, down_full = (
        lax.all_gather(up_weight, "sp", axis=0, tiled=True),
        lax.all_gather(down_weight, "sp", axis=0, tiled=True),
    )
    hidden = jnp.square(
        jax.nn.relu(
            jnp.dot(
                lax.all_gather(normed, "tp", axis=0, tiled=True),
                up_full,
                preferred_element_type=jnp.float32,
            )
        )
    ).astype(jnp.bfloat16)
    ffn = lax.psum_scatter(
        lax.dot_general(
            hidden, down_full, (((1,), (1,)), ((), ())), preferred_element_type=jnp.float32
        ).astype(jnp.bfloat16),
        "tp",
        scatter_dimension=0,
        tiled=True,
    ).astype(jnp.float32)
    return (mixed.astype(jnp.float32) + rms_scale(ffn, ffn_out_gain)).astype(jnp.bfloat16)

lane_tile = 128
row_parts = 2


def attend_rows(qb_ref, qn_ref, lat_ref, kb_ref, vb_ref, kn_ref, vn_ref, o_ref):
    rows = qb_ref.shape[0]
    latent_width = kb_ref.shape[0]
    rope = lat_ref.shape[3] - latent_width
    share = o_ref.shape[1]
    block = 2 * rows
    broad = kb_ref.shape[1] // DB
    narrow = kn_ref.shape[1] // DN
    first = lax.axis_index("sp") * rows
    blocks = lax.div(first + rows + block - 1, block)
    query_pos = first + lax.broadcasted_iota(jnp.int32, (rows, block), 0)
    key_iota = lax.broadcasted_iota(jnp.int32, (rows, block), 1)
    wb = DB + rope
    wn = DN + rope
    heads = broad + narrow
    widths = [DB] * broad + [narrow * DN] * narrow

    def step(index, carried):
        start = pl.multiple_of(index * block, block)
        both = lat_ref[pl.ds(2 * index, 2)].reshape(block, latent_width + rope)
        lat = both[:, :latent_width]
        rot = both[:, latent_width:]

        def expand(ref):
            return jnp.dot(lat, ref[...], preferred_element_type=jnp.float32).astype(jnp.bfloat16)

        kb, vb, kn, vn = expand(kb_ref), expand(vb_ref), expand(kn_ref), expand(vn_ref)
        allowed = key_iota + start <= query_pos
        out = []
        for h in range(heads):
            old_max, old_sum, old_acc = carried[h]
            if h < broad:
                q = qb_ref[:, h * wb : (h + 1) * wb]
                k = jnp.concatenate([kb[:, h * DB : (h + 1) * DB], rot], axis=1)
                v = vb[:, h * DB : (h + 1) * DB]
                scale = wb ** (-0.5)
            else:
                n = h - broad
                q = qn_ref[:, n * wn : (n + 1) * wn]
                k = jnp.concatenate([kn[:, n * DN : (n + 1) * DN], rot], axis=1)
                v = vn
                scale = wn ** (-0.5)
            s = lax.dot_general(
                q, k, (((1,), (1,)), ((), ())), preferred_element_type=jnp.float32
            )
            s = jnp.where(allowed, s * scale, masked_score)
            new_max = jnp.maximum(old_max, jnp.max(s, axis=-1, keepdims=True))
            e = jnp.where(allowed, jnp.exp(s - new_max), 0.0)
            factor = jnp.exp(old_max - new_max)
            new_sum = old_sum * factor + jnp.sum(e, axis=-1, keepdims=True)
            pv = jnp.dot(e.astype(jnp.bfloat16), v, preferred_element_type=jnp.float32)
            out.append((new_max, new_sum, old_acc * factor + pv))
        return tuple(out)

    init = tuple(
        (
            jnp.full((rows, 1), masked_score, jnp.float32),
            jnp.zeros((rows, 1), jnp.float32),
            jnp.zeros((rows, w), jnp.float32),
        )
        for w in widths
    )
    final = lax.fori_loop(0, blocks, step, init)
    parts = [final[h][2] / final[h][1] for h in range(heads)]
    for h in range(broad):
        for t in range(o_ref.shape[0]):
            o_ref[t, :, h * DB : (h + 1) * DB] = parts[h][t * share : (t + 1) * share].astype(
                o_ref.dtype
            )
    if narrow:
        column = lax.broadcasted_iota(jnp.int32, parts[broad].shape, 1)
        mixed = parts[broad]
        for n in range(1, narrow):
            mixed = jnp.where(column >= n * DN, parts[broad + n], mixed)
        for t in range(o_ref.shape[0]):
            o_ref[t, :, broad * DB :] = mixed[t * share : (t + 1) * share].astype(o_ref.dtype)


def layer_kernel(
    sp,
    tp,
    mine_ref,
    qb_ref,
    qn_ref,
    resid_ref,
    kb_ref,
    vb_ref,
    kn_ref,
    vn_ref,
    ob_hbm,
    on_hbm,
    post_ref,
    gain_ref,
    last_ref,
    up_hbm,
    down_hbm,
    out_ref,
    lat,
    attn,
    heads,
    ob,
    on,
    up,
    down,
    rows,
    total,
    core_send,
    core_got,
    x_send,
    x_got,
    z_send,
    z_got,
    send_sem,
    recv_sem,
    local_sem,
):
    cols = row_parts
    lines = sp // cols
    s = lax.axis_index("sp")
    t = lax.axis_index("tp")
    z = s // cols
    y = s % cols
    core = t % 2
    ports = t // 2
    t_core = t + 1 - 2 * core
    t_x = (1 - ports) * 2 + core
    t_both = (1 - ports) * 2 + (1 - core)
    s_y = z * cols + 1 - y
    bf16 = jnp.bfloat16
    share = resid_ref.shape[0]
    width = up.shape[2]

    def line(k):
        return (z + k + lines) % lines * cols + y

    def source(k, flipped):
        return (z - k + lines) % lines * cols + ((1 - y) if flipped else y)

    peers = [(line(k), t) for k in range(1, lines)]
    peers += [(s_y, t), (s, t_core), (s, t_x), (s, t_both)]
    barrier = pltpu.get_barrier_semaphore()
    for peer in peers:
        pl.semaphore_signal(
            barrier, inc=1, device_id=peer, device_id_type=pl.DeviceIdType.MESH
        )
    pl.semaphore_wait(barrier, len(peers))

    started = []

    def send(src, dst, peer):
        i = len(started)
        copy = pltpu.make_async_remote_copy(
            src_ref=src,
            dst_ref=dst,
            send_sem=send_sem.at[i],
            recv_sem=recv_sem.at[i],
            device_id=peer,
            device_id_type=pl.DeviceIdType.MESH,
        )
        copy.start()
        started.append(copy)
        return copy

    locals_ = []

    def bring(src, dst):
        copy = pltpu.make_async_copy(src, dst, local_sem.at[len(locals_)])
        copy.start()
        locals_.append(copy)
        return copy

    def cut(ref, k):
        at = pl.multiple_of((z + k) % lines * width, width)
        return ref.at[:, pl.ds(at, width)]

    far = list(range(1, lines))
    lat_z = {k: send(mine_ref, lat.at[s, core], (line(k), t)) for k in far}
    lat_y = {0: send(mine_ref, lat.at[s, core], (s_y, t))}
    lat_c = [send(mine_ref, lat.at[s, core], (s, t_core))]
    up_z = {k: send(cut(up_hbm, k), up.at[s], (line(k), t)) for k in far}
    down_z = {k: send(cut(down_hbm, k), down.at[s], (line(k), t)) for k in far}
    own = [bring(cut(up_hbm, 0), up.at[s]), bring(cut(down_hbm, 0), down.at[s])]
    outs = [bring(ob_hbm, ob), bring(on_hbm, on)]
    lat[s, core] = mine_ref[...]
    order = sorted(far, key=lambda k: min(k, lines - k))
    for k in order:
        lat_z[k].wait_recv()
        held = lat.at[source(k, False), core]
        lat_y[k] = send(held, held, (s_y, t))
        lat_c.append(send(held, held, (s, t_core)))
    for k in [0] + order:
        lat_y[k].wait_recv()
        held = lat.at[source(k, True), core]
        lat_c.append(send(held, held, (s, t_core)))
    up_y = [send(cut(up_hbm, 0), up.at[s], (s_y, t))]
    down_y = [send(cut(down_hbm, 0), down.at[s], (s_y, t))]
    for copy in lat_c:
        copy.wait_recv()

    attend_rows(qb_ref, qn_ref, lat, kb_ref, vb_ref, kn_ref, vn_ref, attn)

    moved = [
        send(attn.at[peer], heads.at[t], (s, peer)) for peer in (t_x, t_both, t_core)
    ]
    heads[t] = attn[t]
    for k in order:
        up_z[k].wait_recv()
        held = up.at[source(k, False)]
        up_y.append(send(held, held, (s_y, t)))
    for copy in outs:
        copy.wait()
    for copy in moved:
        copy.wait_recv()

    broad_width = kb_ref.shape[1]
    narrow_width = kn_ref.shape[1]
    projected = jnp.zeros((share, ob.shape[1]), jnp.float32)
    for i in range(tp):
        projected = projected + jnp.dot(
            heads[i, :, :broad_width],
            ob[i * broad_width : (i + 1) * broad_width],
            preferred_element_type=jnp.float32,
        )
        projected = projected + jnp.dot(
            heads[i, :, broad_width:],
            on[i * narrow_width : (i + 1) * narrow_width],
            preferred_element_type=jnp.float32,
        )
    mixed = (
        resid_ref[...].astype(jnp.float32) + rms_scale(projected, post_ref[...])
    ).astype(bf16)
    rows[0, 0] = rms_scale(mixed.astype(jnp.float32), gain_ref[...]).astype(bf16)

    row_z = {k: send(rows.at[0, 0], rows.at[0, k], (line(k), t)) for k in far}
    row_x = {0: send(rows.at[0, 0], rows.at[1, 0], (s, t_x))}
    row_c = {0: send(rows.at[0, 0], rows.at[2, 0], (s, t_core))}
    row_b = {}
    for k in order:
        down_z[k].wait_recv()
        held = down.at[source(k, False)]
        down_y.append(send(held, held, (s_y, t)))
    row_x[0].wait_recv()
    row_b[0] = send(rows.at[1, 0], rows.at[3, 0], (s, t_core))
    for k in order:
        row_z[k].wait_recv()
        row_x[k] = send(rows.at[0, k], rows.at[1, k], (s, t_x))
        row_c[k] = send(rows.at[0, k], rows.at[2, k], (s, t_core))
    for copy in own:
        copy.wait()
    for copy in up_y + down_y:
        copy.wait_recv()

    deep = sp * up.shape[1]

    def feed(j):
        block = rows[j].reshape(lines * share, rows.shape[3])
        product = jnp.dot(block, up[...].reshape(deep, width), preferred_element_type=jnp.float32)
        hidden = jnp.square(jnp.maximum(product, 0.0)).astype(bf16)
        return lax.dot_general(
            hidden,
            down[...].reshape(deep, width),
            (((1,), (1,)), ((), ())),
            preferred_element_type=jnp.float32,
        )

    total[0] = feed(0)
    for k in [0] + order:
        row_c[k].wait_recv()
    core_send[0] = feed(2).astype(bf16)
    sum_c = [send(core_send.at[0], core_got.at[0], (s, t_core))]
    for k in order:
        row_x[k].wait_recv()
        row_b[k] = send(rows.at[1, k], rows.at[3, k], (s, t_core))
    total[1] = feed(1)
    for k in [0] + order:
        row_b[k].wait_recv()
    core_send[1] = feed(3).astype(bf16)
    sum_c.append(send(core_send.at[1], core_got.at[1], (s, t_core)))
    sum_c[1].wait_recv()
    sum_x = {}
    back = order[::-1] + [0]
    for k in back:
        part = slice(k * share, (k + 1) * share)
        x_send[k] = (total[1, part] + core_got[1, part].astype(jnp.float32)).astype(bf16)
        sum_x[k] = send(x_send.at[k], x_got.at[k], (s, t_x))
    sum_c[0].wait_recv()
    sum_z = []
    for k in back:
        part = slice(k * share, (k + 1) * share)
        sum_x[k].wait_recv()
        piece = (
            total[0, part]
            + core_got[0, part].astype(jnp.float32)
            + x_got[k].astype(jnp.float32)
        )
        if k:
            z_send[k] = piece.astype(bf16)
            sum_z.append(send(z_send.at[k], z_got.at[k], (line(-k), t)))
        else:
            ffn = piece
    for copy in sum_z:
        copy.wait_recv()
    for k in far:
        ffn = ffn + z_got[k].astype(jnp.float32)
    out_ref[...] = (mixed.astype(jnp.float32) + rms_scale(ffn, last_ref[...])).astype(bf16)
    for copy in started:
        copy.wait_send()


def fast_local(
    resid,
    query_broad,
    query_narrow,
    latent,
    key_rope,
    latent_gain,
    key_up_broad,
    value_up_broad,
    key_up_narrow,
    value_up_narrow,
    out_broad,
    out_narrow,
    post_gain,
    ffn_gain,
    up_weight,
    down_weight,
    ffn_out_gain,
):
    sp = lax.axis_size("sp")
    tp = lax.axis_size("tp")
    cols = row_parts
    lines = sp // cols
    s = lax.axis_index("sp")
    z = s // cols
    y = s % cols
    local_rows = resid.shape[0]
    share_rows = local_rows // tp
    query_pos = s * local_rows + jnp.arange(local_rows, dtype=jnp.int32)
    rope_width = key_rope.shape[1]
    bf16 = jnp.bfloat16

    normed_latent = rms_scale(latent.astype(jnp.float32), latent_gain).astype(bf16)
    key_rot = rotate(key_rope.astype(jnp.float32), query_pos).astype(bf16)
    both = jnp.concatenate([normed_latent, key_rot], axis=1)
    core = lax.axis_index("tp") % 2
    half_rows = local_rows // 2
    mine = lax.dynamic_slice_in_dim(both, core * half_rows, half_rows, 0)
    def rotate_queries(queries, head_size):
        parts = queries.reshape(local_rows, -1, head_size + rope_width)
        rotated = rotate(parts[:, :, head_size:].astype(jnp.float32), query_pos).astype(bf16)
        return jnp.concatenate([parts[:, :, :head_size], rotated], axis=-1).reshape(queries.shape)

    broad_width = key_up_broad.shape[1]
    narrow_width = key_up_narrow.shape[1]
    width = broad_width + narrow_width
    deep = resid.shape[1]
    slice_width = up_weight.shape[1] // lines
    own_resid = lax.dynamic_slice_in_dim(resid, lax.axis_index("tp") * share_rows, share_rows, 0)
    vmem = pl.BlockSpec(memory_space=pltpu.VMEM)
    anywhere = pl.BlockSpec(memory_space=pl.ANY)
    return pl.pallas_call(
        functools.partial(layer_kernel, sp, tp),
        out_shape=jax.ShapeDtypeStruct((share_rows, deep), bf16),
        in_specs=[vmem] * 8 + [anywhere] * 2 + [vmem] * 3 + [anywhere] * 2,
        out_specs=vmem,
        scratch_shapes=[
            pltpu.VMEM((sp, 2, half_rows, both.shape[1]), bf16),
            pltpu.VMEM((tp, share_rows, width), bf16),
            pltpu.VMEM((tp, share_rows, width), bf16),
            pltpu.VMEM(out_broad.shape, bf16),
            pltpu.VMEM(out_narrow.shape, bf16),
            pltpu.VMEM((sp, up_weight.shape[0], slice_width), bf16),
            pltpu.VMEM((sp, up_weight.shape[0], slice_width), bf16),
            pltpu.VMEM((tp, lines, share_rows, deep), bf16),
            pltpu.VMEM((2, lines * share_rows, deep), jnp.float32),
            pltpu.VMEM((2, lines * share_rows, deep), bf16),
            pltpu.VMEM((2, lines * share_rows, deep), bf16),
            pltpu.VMEM((lines, share_rows, deep), bf16),
            pltpu.VMEM((lines, share_rows, deep), bf16),
            pltpu.VMEM((lines, share_rows, deep), bf16),
            pltpu.VMEM((lines, share_rows, deep), bf16),
            pltpu.SemaphoreType.DMA((15 * lines + 2,)),
            pltpu.SemaphoreType.DMA((15 * lines + 2,)),
            pltpu.SemaphoreType.DMA((4,)),
        ],
        compiler_params=pltpu.CompilerParams(
            collective_id=0, has_side_effects=True, vmem_limit_bytes=60 * 2**20
        ),
    )(
        mine,
        rotate_queries(query_broad, DB),
        rotate_queries(query_narrow, DN),
        own_resid,
        key_up_broad,
        value_up_broad,
        key_up_narrow,
        value_up_narrow,
        out_broad,
        out_narrow,
        post_gain[None],
        ffn_gain[None],
        ffn_out_gain[None],
        up_weight,
        down_weight,
    )


def solution(mesh):
    in_specs = (
        P("sp", None),
        P("sp", "tp"),
        P("sp", "tp"),
        P("sp", None),
        P("sp", None),
        P(),
        P(None, "tp"),
        P(None, "tp"),
        P(None, "tp"),
        P(None, "tp"),
        P(),
        P(),
        P(),
        P(),
        P("sp", "tp"),
        P("sp", "tp"),
        P(),
    )
    out_specs = P(("sp", "tp"), None)
    sp = mesh.shape["sp"]
    tp = mesh.shape["tp"]

    def whole(*args):
        hidden = args[14].shape[1] // tp
        rows = args[0].shape[0] // sp
        lines = sp // row_parts
        fits = (
            sp % row_parts == 0
            and tp & (tp - 1) == 0
            and tp == 4
            and lines > 1
            and hidden % (lines * lane_tile) == 0
            and rows % (16 * tp) == 0
        )
        body = fast_local if fits else local
        return jax.shard_map(
            body, mesh=mesh, in_specs=in_specs, out_specs=out_specs, check_vma=False
        )(*args)

    return whole
```

profile of v0, /device:TPU:0, one launch (start us, length us, event | category | flops | bytes accessed | tf_op | source)
XLA Modules:
  0.0 129.7 jit_solution(16614896853915791879)
XLA Ops:
  0.0 0.0 copy-start
  0.0 0.9 copy.19
  1.0 0.5 multiply_cosine_fusion
  1.4 1.0 fusion
  2.5 1.0 fusion.2
  3.6 0.7 fusion.4.mine_ref
  4.3 1.1 reshape.82
  5.4 0.9 reshape.84
  6.3 0.3 fusion.5
  6.5 0.6 subtract_convert_fusion
  7.1 0.4 pad_maximum_fusion.1
  7.6 0.7 copy.23
  8.2 0.1 slice.42
  8.3 0.4 pad_maximum_fusion
  8.7 0.8 reshape.83.qb_ref
  9.5 0.0 copy-done
  9.5 0.7 constant_dynamic-slice_fusion.resid_ref
  10.2 117.9 %shard_map.163 = bf16[48,2048]{1,0:T(8,128)(2,1)} custom-call(bf16[96,576]{1,0:T(8,128)(2,1)} %fusion.4.mine_ref, bf16[192,384]{1,0:T(8,128)(2,1)} %reshape.83.qb_ref, bf16[192,256]{1,0:T(8,128)(2,1)} %bitcast.7, bf16[48,2048]{1,0:T(8,128)(2,1)} %constant_dynamic-slice_fusion.resid_ref, bf16[512,256]{1,0:T(8,128)(2,1)} %kb_ref.1, bf16[512,256]{1,0:T(8,128)(2,1)} %vb_ref.1, ...), custom_call_target="tpu_custom_call" | custom-call | tf_op jit(solution)/shard_map/pallas_call | solution.py:571
  128.1 1.6 %copy.25 = bf16[48,2048]{1,0:T(8,128)(2,1)} copy(bf16[48,2048]{1,0:T(8,128)(2,1)} %shard_map.163) | data formatting | bytes 393216
  (4 shorter events, 0.0 us)
Async XLA Ops:
  0.0 9.5 %copy-start = (bf16[192,2048]{1,0:T(8,128)(2,1)S(1)}, bf16[192,2048]{1,0:T(8,128)(2,1)}, u32[]{:S(2)}) copy-start(bf16[192,2048]{1,0:T(8,128)(2,1)} %param.17) | copy-start | bytes 2359300
where the time goes:
time: 130 us
  Pallas kernels  118 us (91%)
  local copies, waits for them, and re-layouts  6.77 us (5%)
  other arithmetic  4.94 us (4%)
    pallas_call x1, Pallas kernels, fast_local(): pl.pallas_call(functools.partial(layer_kernel, sp, tp), out_shape=jax.Sha...  118 us
    unnamed x5, local copies, waits for them, and re-layouts  3.22 us

commit v1 on v0

--- a/solution.py
+++ b/solution.py
@@ -289,9 +289,12 @@
 def layer_kernel(
     sp,
     tp,
-    mine_ref,
-    qb_ref,
-    qn_ref,
+    latent_ref,
+    key_rope_ref,
+    table_ref,
+    latent_gain_ref,
+    qb_in,
+    qn_in,
     resid_ref,
     kb_ref,
     vb_ref,
@@ -305,6 +308,9 @@
     up_hbm,
     down_hbm,
     out_ref,
+    mine_ref,
+    qb_ref,
+    qn_ref,
     lat,
     attn,
     heads,
@@ -337,7 +343,7 @@
     t_both = (1 - ports) * 2 + (1 - core)
     s_y = z * cols + 1 - y
     bf16 = jnp.bfloat16
-    share = resid_ref.shape[0]
+    share = resid_ref.shape[0] // tp
     width = up.shape[2]
 
     def line(k):
@@ -353,6 +359,22 @@
         pl.semaphore_signal(
             barrier, inc=1, device_id=peer, device_id_type=pl.DeviceIdType.MESH
         )
+
+    rope = key_rope_ref.shape[1]
+    half_rope = rope // 2
+
+    def turn(values, table):
+        values = values.astype(jnp.float32)
+        swapped = jnp.concatenate([values[:, half_rope:], values[:, :half_rope]], axis=1)
+        return (values * table[:, :rope] + swapped * table[:, rope:]).astype(bf16)
+
+    latent_width = latent_ref.shape[1]
+    half = mine_ref.shape[0]
+    mine_rows = pl.ds(pl.multiple_of(core * half, 16), half)
+    mine_ref[:, :latent_width] = rms_scale(
+        latent_ref[mine_rows, :].astype(jnp.float32), latent_gain_ref[...]
+    ).astype(bf16)
+    mine_ref[:, latent_width:] = turn(key_rope_ref[mine_rows, :], table_ref[mine_rows, :])
     pl.semaphore_wait(barrier, len(peers))
 
     started = []
@@ -392,6 +414,14 @@
     own = [bring(cut(up_hbm, 0), up.at[s]), bring(cut(down_hbm, 0), down.at[s])]
     outs = [bring(ob_hbm, ob), bring(on_hbm, on)]
     lat[s, core] = mine_ref[...]
+    for queries, turned, size in ((qb_in, qb_ref, DB), (qn_in, qn_ref, DN)):
+        step = size + rope
+        for h in range(queries.shape[1] // step):
+            middle = h * step + size
+            turned[:, h * step : middle] = queries[:, h * step : middle]
+            turned[:, middle : middle + rope] = turn(
+                queries[:, middle : middle + rope], table_ref[...]
+            )
     order = sorted(far, key=lambda k: min(k, lines - k))
     for k in order:
         lat_z[k].wait_recv()
@@ -437,7 +467,8 @@
             preferred_element_type=jnp.float32,
         )
     mixed = (
-        resid_ref[...].astype(jnp.float32) + rms_scale(projected, post_ref[...])
+        resid_ref[pl.ds(pl.multiple_of(t * share, 16), share), :].astype(jnp.float32)
+        + rms_scale(projected, post_ref[...])
     ).astype(bf16)
     rows[0, 0] = rms_scale(mixed.astype(jnp.float32), gain_ref[...]).astype(bf16)
 
@@ -549,32 +580,29 @@
     rope_width = key_rope.shape[1]
     bf16 = jnp.bfloat16
 
-    normed_latent = rms_scale(latent.astype(jnp.float32), latent_gain).astype(bf16)
-    key_rot = rotate(key_rope.astype(jnp.float32), query_pos).astype(bf16)
-    both = jnp.concatenate([normed_latent, key_rot], axis=1)
-    core = lax.axis_index("tp") % 2
+    frequency = rope_base ** (-2.0 * jnp.arange(rope_width // 2, dtype=jnp.float32) / rope_width)
+    angles = query_pos.astype(jnp.float32)[:, None] * frequency[None, :]
+    cosine, sine = jnp.cos(angles), jnp.sin(angles)
+    table = jnp.concatenate([cosine, cosine, -sine, sine], axis=1)
     half_rows = local_rows // 2
-    mine = lax.dynamic_slice_in_dim(both, core * half_rows, half_rows, 0)
-    def rotate_queries(queries, head_size):
-        parts = queries.reshape(local_rows, -1, head_size + rope_width)
-        rotated = rotate(parts[:, :, head_size:].astype(jnp.float32), query_pos).astype(bf16)
-        return jnp.concatenate([parts[:, :, :head_size], rotated], axis=-1).reshape(queries.shape)
-
+    both_width = latent.shape[1] + rope_width
     broad_width = key_up_broad.shape[1]
     narrow_width = key_up_narrow.shape[1]
     width = broad_width + narrow_width
     deep = resid.shape[1]
     slice_width = up_weight.shape[1] // lines
-    own_resid = lax.dynamic_slice_in_dim(resid, lax.axis_index("tp") * share_rows, share_rows, 0)
     vmem = pl.BlockSpec(memory_space=pltpu.VMEM)
     anywhere = pl.BlockSpec(memory_space=pl.ANY)
     return pl.pallas_call(
         functools.partial(layer_kernel, sp, tp),
         out_shape=jax.ShapeDtypeStruct((share_rows, deep), bf16),
-        in_specs=[vmem] * 8 + [anywhere] * 2 + [vmem] * 3 + [anywhere] * 2,
+        in_specs=[vmem] * 11 + [anywhere] * 2 + [vmem] * 3 + [anywhere] * 2,
         out_specs=vmem,
         scratch_shapes=[
-            pltpu.VMEM((sp, 2, half_rows, both.shape[1]), bf16),
+            pltpu.VMEM((half_rows, both_width), bf16),
+            pltpu.VMEM(query_broad.shape, bf16),
+            pltpu.VMEM(query_narrow.shape, bf16),
+            pltpu.VMEM((sp, 2, half_rows, both_width), bf16),
             pltpu.VMEM((tp, share_rows, width), bf16),
             pltpu.VMEM((tp, share_rows, width), bf16),
             pltpu.VMEM(out_broad.shape, bf16),
@@ -597,10 +625,13 @@
             collective_id=0, has_side_effects=True, vmem_limit_bytes=60 * 2**20
         ),
     )(
-        mine,
-        rotate_queries(query_broad, DB),
-        rotate_queries(query_narrow, DN),
-        own_resid,
+        latent,
+        key_rope,
+        table,
+        latent_gain[None],
+        query_broad,
+        query_narrow,
+        resid,
         key_up_broad,
         value_up_broad,
         key_up_narrow,

time: 130 us -> 123 us (0.946)
  other arithmetic: 4.94 us -> 1.23 us
  local copies, waits for them, and re-layouts: 6.77 us -> 3.09 us
    reshape x3 -> x0, local copies, waits for them, and re-layouts: 2.79 us -> none  [the longest x2 1.99 us: rotate_queries(): parts = queries.reshape(local_rows, -1, head_size + rope_width)]
    unnamed x5 -> x2, local copies, waits for them, and re-layouts: 3.22 us -> 3.09 us
where the time goes in v1:
time: 123 us; the launch traced here: 122 us
  Pallas kernels  118 us (96%)
  local copies, waits for them, and re-layouts  3.09 us (3%)
  other arithmetic  1.23 us (1%)
    pallas_call x1, Pallas kernels, fast_local(): pl.pallas_call(functools.partial(layer_kernel, sp, tp), out_shape=jax.Sha...  118 us
    unnamed x2, local copies, waits for them, and re-layouts  3.09 us

profile of v1, /device:TPU:0, one launch (start us, length us, event | category | flops | bytes accessed | tf_op | source)
XLA Modules:
  0.0 122.5 jit_solution(2693479296884755846)
XLA Ops:
  0.0 0.4 multiply_cosine_fusion
  0.4 0.8 pad_maximum_fusion.table_ref
  1.2 1.5 %copy.20.key_rope_ref = bf16[192,64]{1,0:T(8,128)(2,1)} copy(bf16[192,64]{0,1:T(8,128)(2,1)} %param.21) | data formatting | bytes 49152 | tf_op args[4]
  2.7 118.1 %shard_map.163 = bf16[48,2048]{1,0:T(8,128)(2,1)} custom-call(bf16[192,512]{1,0:T(8,128)(2,1)} %latent_ref.1, bf16[192,64]{1,0:T(8,128)(2,1)} %copy.20.key_rope_ref, f32[192,128]{1,0:T(8,128)} %pad_maximum_fusion.table_ref, f32[1,512]{1,0:T(1,128)} %bitcast.7, bf16[192,384]{1,0:T(8,128)(2,1)} %qb_in.1, bf16[192,256]{1,0:T(8,128)(2,1)} %qn_in.1, ...), custom_call_target="tpu_custom_call" | custom-call | tf_op jit(solution)/shard_map/pallas_call | solution.py:596
  120.8 1.6 %copy.22 = bf16[48,2048]{1,0:T(8,128)(2,1)} copy(bf16[48,2048]{1,0:T(8,128)(2,1)} %shard_map.163) | data formatting | bytes 393216
  (2 shorter events, 0.0 us)
